TPU v7x, 32 devices: a whole 2x2x4 slice. The times are simulated.
32 devices in a mesh: ep: 4 (over y, x), tp: 8 (over z, core).
Axes of the slice: x: 2, y: 2, z: 4, core: 2. Of those that a mesh axis runs over, the one named last changes fastest.
Arguments:
- tokens: bfloat16 [64, 2048], P('ep', 'tp'), may hold values from -6 to 6
- key_cache: bfloat16 [64, 16, 1024, 128], P('ep', 'tp'), may hold values from -1700 to 1700
- value_cache: bfloat16 [64, 16, 1024, 128], P('ep', 'tp'), may hold values from -6 to 6
- gate_totals: float32 [64, 16, 1024], P('ep', 'tp'), as said below
- lengths: int32 [64], P('ep'), may hold values from 128 to 1024
- attn_gain: float32 [2048], replicated, may hold values from 0.1 to 1.9
- w_query: bfloat16 [2048, 2048], P(None, 'tp'), may hold values from -0.125 to 0.125
- w_key: bfloat16 [2048, 2048], P(None, 'tp'), may hold values from -0.125 to 0.125
- w_value: bfloat16 [2048, 2048], P(None, 'tp'), may hold values from -0.125 to 0.125
- w_forget: bfloat16 [2048, 16], replicated, may hold values from -0.125 to 0.125
- forget_bias: float32 [16], replicated, may hold values from -3 to 0
- w_attn_out: bfloat16 [2048, 2048], P('tp'), may hold values from -0.1875 to 0.1875
- moe_gain: float32 [2048], replicated, may hold values from 0.1 to 1.9
- group_ids: int32 [64, 1], P('ep'), may hold values from 0 to 3; in each aligned block of 16 rows (0 to 15, 16 to 31, ...) at most 8 rows name the same one
- inner_ids: int32 [64, 2], P('ep'), may hold values from 0 to 3, all different within a row
- group_prob: float32 [64], P('ep'), may hold values from 0.2 to 1
- pair_logits: float32 [64, 2], P('ep'), may hold values from -6 to 6
- w_expert_gate: bfloat16 [4, 2048, 2048], P('ep', None, 'tp'), may hold values from -0.125 to 0.125
- w_expert_up: bfloat16 [4, 2048, 2048], P('ep', None, 'tp'), may hold values from -0.125 to 0.125
- w_expert_down: bfloat16 [4, 2048, 2048], P('ep', 'tp'), may hold values from -0.375 to 0.375
- w_dense_in: bfloat16 [2048, 2048], P(None, 'tp'), may hold values from -0.125 to 0.125
- w_dense_out: bfloat16 [2048, 2048], P('tp'), may hold values from -0.1875 to 0.1875
- dense_gate: float32 [2048], P('tp'), may hold values from -2 to 2
Outputs:
- layer_output: bfloat16 [64, 2048], P('ep', 'tp')
- new_keys: bfloat16 [64, 16, 128], P('ep', 'tp')
- new_values: bfloat16 [64, 16, 128], P('ep', 'tp')
- new_gates: float32 [64, 16], P('ep', 'tp')
Inputs may be any that keep to these rules, and one draw needn't show every extreme that they name: `group_ids`: within the 16 sequences of each index of ep (aligned blocks of rows), no group is named by more than 8 sequences, a bound that some block reaches. `inner_ids`: each row names 2 different experts of its group. `gate_totals`: along positions the values of each sequence and head never rise.
All inputs are finite; a program needn't handle non-finite values.
Results may differ from a plain program's by a relative error of at most 0.011.
Values may be sent and summed in bfloat16 or wider, within the bound.
A program may use at most 64 MiB of HBM per device.

v0:
```python
import jax
import jax.numpy as jnp
from jax import lax
from jax.sharding import PartitionSpec as P

FFE = 512
EPG = 4
EPS = 1e-06
FLOOR = -1e30


def norm_rows(row_data, gain_vec):
    values = row_data.astype(jnp.float32)
    factor = lax.rsqrt(jnp.mean(values * values, axis=-1, keepdims=True) + EPS)
    return (values * factor * gain_vec).astype(jnp.bfloat16)


def head_norm(values):
    factor = lax.rsqrt(jnp.mean(values * values, axis=-1, keepdims=True) + EPS)
    return (values * factor).astype(jnp.bfloat16)


def attend(queries, fresh_key, fresh_value, key_cache, value_cache, gate_totals, lengths, current):
    score_scale = queries.shape[-1] ** (-0.5)
    scores = (
        jnp.einsum("shd,shld->shl", queries, key_cache, preferred_element_type=jnp.float32)
        * score_scale
    )
    scores = scores + current[:, :, None] - gate_totals
    entry_indices = jnp.arange(key_cache.shape[2])
    live_mask = (entry_indices[None, :] < lengths[:, None])[:, None, :]
    scores = jnp.where(live_mask, scores, FLOOR)
    own_score = (
        jnp.sum(queries.astype(jnp.float32) * fresh_key.astype(jnp.float32), axis=-1) * score_scale
    )
    peak = jnp.maximum(jnp.max(scores, axis=-1), own_score)
    expo_terms = jnp.where(live_mask, jnp.exp(scores - peak[:, :, None]), 0.0)
    own_expo = jnp.exp(own_score - peak)
    denom_sum = jnp.sum(expo_terms, axis=-1) + own_expo
    weights = (expo_terms / denom_sum[:, :, None]).astype(jnp.bfloat16)
    own_weight = (own_expo / denom_sum).astype(jnp.bfloat16)
    attended = jnp.einsum("shl,shld->shd", weights, value_cache, preferred_element_type=jnp.float32)
    attended = attended + own_weight.astype(jnp.float32)[:, :, None] * fresh_value.astype(
        jnp.float32
    )
    return attended.astype(jnp.bfloat16)


def body(
    tokens,
    key_cache,
    value_cache,
    gate_totals,
    lengths,
    attn_gain,
    w_query,
    w_key,
    w_value,
    w_forget,
    forget_bias,
    w_attn_out,
    moe_gain,
    group_ids,
    inner_ids,
    group_prob,
    pair_logits,
    w_expert_gate,
    w_expert_up,
    w_expert_down,
    w_dense_in,
    w_dense_out,
    dense_gate,
):
    gathered = lax.all_gather(tokens, "tp", axis=1, tiled=True)
    normed = norm_rows(gathered, attn_gain)
    seq_count = gathered.shape[0]
    heads_dev = key_cache.shape[1]
    head_dim = key_cache.shape[3]

    def project(weight):
        return jnp.dot(normed, weight, preferred_element_type=jnp.float32).reshape(
            seq_count, heads_dev, head_dim
        )

    queries = head_norm(project(w_query))
    new_keys = head_norm(project(w_key))
    new_values = project(w_value).astype(jnp.bfloat16)
    first_head = lax.axis_index("tp") * heads_dev
    forget_cols = lax.dynamic_slice_in_dim(w_forget, first_head, heads_dev, 1)
    forget_shift = lax.dynamic_slice_in_dim(forget_bias, first_head, heads_dev, 0)
    log_gate = jax.nn.log_sigmoid(
        jnp.dot(normed, forget_cols, preferred_element_type=jnp.float32) + forget_shift
    )
    entry_indices = jnp.arange(gate_totals.shape[2])
    at_last = (entry_indices[None, :] == (lengths - 1)[:, None])[:, None, :]
    new_gates = jnp.sum(jnp.where(at_last, gate_totals, 0.0), axis=2) + log_gate
    attended = attend(
        queries, new_keys, new_values, key_cache, value_cache, gate_totals, lengths, new_gates
    )
    partial_value = jnp.dot(
        attended.reshape(seq_count, heads_dev * head_dim),
        w_attn_out,
        preferred_element_type=jnp.float32,
    )
    piece_sum = lax.psum_scatter(partial_value, "tp", scatter_dimension=1, tiled=True)
    own_residual = (tokens.astype(jnp.float32) + piece_sum).astype(jnp.bfloat16)
    moe_in = norm_rows(lax.all_gather(own_residual, "tp", axis=1, tiled=True), moe_gain)
    groups = lax.axis_size("ep")
    capacity = max(2, 2 * seq_count // groups)
    first_share = jax.nn.sigmoid(pair_logits[:, 0] - pair_logits[:, 1])
    pair_share = group_prob[:, None] * jnp.stack([first_share, 1.0 - first_share], axis=1)
    inner_range = jnp.arange(EPG)
    spread = jnp.sum(
        jnp.where(inner_ids[:, :, None] == inner_range[None, None, :], pair_share[:, :, None], 0.0),
        axis=1,
    ).astype(jnp.bfloat16)
    choose = (group_ids == jnp.arange(groups)[None, :]).astype(jnp.int32)
    before = jnp.cumsum(choose, axis=0) - choose
    slot_of = group_ids[:, 0] * capacity + jnp.sum(before * choose, axis=1)
    slot_ids = jnp.arange(groups * capacity)
    send_map = (slot_of[None, :] == slot_ids[:, None]).astype(jnp.bfloat16)
    send_weights = jnp.dot(send_map, spread, preferred_element_type=jnp.float32).astype(
        jnp.bfloat16
    )
    send_rows = jnp.dot(send_map, moe_in, preferred_element_type=jnp.float32).astype(jnp.bfloat16)
    recv_rows, recv_weights = (
        lax.all_to_all(send_rows, "ep", split_axis=0, concat_axis=0, tiled=True),
        lax.all_to_all(send_weights, "ep", split_axis=0, concat_axis=0, tiled=True),
    )
    dense_hidden = jax.nn.silu(
        jnp.dot(moe_in, w_dense_in, preferred_element_type=jnp.float32)
    ).astype(jnp.bfloat16)
    dense_part = jnp.dot(dense_hidden, w_dense_out, preferred_element_type=jnp.float32)
    hidden_dev = w_expert_gate.shape[2]
    expert_index = lax.axis_index("tp") * hidden_dev // FFE
    route_col = jnp.sum(
        jnp.where(inner_range[None, :] == expert_index, recv_weights.astype(jnp.float32), 0.0),
        axis=1,
    )
    gate_pre = jnp.dot(recv_rows, w_expert_gate[0], preferred_element_type=jnp.float32)
    up_pre = jnp.dot(recv_rows, w_expert_up[0], preferred_element_type=jnp.float32)
    hidden = (jax.nn.silu(gate_pre) * up_pre * route_col[:, None]).astype(jnp.bfloat16)
    expert_part = jnp.dot(hidden, w_expert_down[0], preferred_element_type=jnp.float32)
    expert_sum, dense_sum = (
        lax.psum_scatter(expert_part, "tp", scatter_dimension=1, tiled=True),
        lax.psum_scatter(dense_part, "tp", scatter_dimension=1, tiled=True),
    )
    returned = lax.all_to_all(
        expert_sum.astype(jnp.bfloat16), "ep", split_axis=0, concat_axis=0, tiled=True
    )
    expert_out = lax.dot_general(
        send_map, returned, (((0,), (0,)), ((), ())), preferred_element_type=jnp.float32
    )
    layer_output = (
        own_residual.astype(jnp.float32) + expert_out + jax.nn.sigmoid(dense_gate) * dense_sum
    )
    return (layer_output.astype(jnp.bfloat16), new_keys, new_values, new_gates)


def solution(mesh):
    placed = (
        P("ep", "tp"),
        P("ep", "tp", None, None),
        P("ep", "tp", None, None),
        P("ep", "tp", None),
        P("ep"),
        P(),
        P(None, "tp"),
        P(None, "tp"),
        P(None, "tp"),
        P(),
        P(),
        P("tp", None),
        P(),
        P("ep", None),
        P("ep", None),
        P("ep"),
        P("ep", None),
        P("ep", None, "tp"),
        P("ep", None, "tp"),
        P("ep", "tp", None),
        P(None, "tp"),
        P("tp", None),
        P("tp"),
    )
    return jax.shard_map(
        body,
        mesh=mesh,
        in_specs=placed,
        out_specs=(P("ep", "tp"), P("ep", "tp", None), P("ep", "tp", None), P("ep", "tp")),
        check_vma=False,
    )
```

profile of v0, /device:TPU:0, one launch (start us, length us, event | category | flops | bytes accessed | tf_op | source)
XLA Modules:
  0.0 172.8 jit_solution(14352880859179264883)
XLA Ops:
  7.2 0.0 copy-start
  7.2 0.0 copy-start.5
  7.2 0.0 copy-start.4
  7.2 0.0 reduce-scatter.4.cloned.1.call-start
  7.3 0.8 broadcast_add_fusion
  8.1 0.7 iota_compare_fusion.1
  8.8 15.9 %all_gather.6 = bf16[16,2048]{1,0:T(8,128)(2,1)S(1)} all-gather(bf16[16,256]{1,0:T(8,128)(2,1)} %param.23), channel_id=1, replica_groups=mesh['ep'=4,'tp'=8] {'tp'}, dimensions={1}, use_global_device_ids=true | all-gather | bytes 73728 | tf_op jit(solution)/shard_map/all_gather | solution.py:74
  24.7 0.1 fusion.12
  24.8 1.5 fusion.67
  26.4 0.1 multiply_reduce_fusion.1
  26.5 1.5 fusion.70
  28.0 0.1 multiply_reduce_fusion.2
  28.1 0.1 iota_compare_fusion
  28.2 1.1 select_reduce_fusion
  29.3 0.1 copy.45
  29.4 0.7 dynamic_slice.7
  30.1 1.0 fusion.58
  31.1 0.0 copy-start.11
  31.1 0.1 copy.46
  31.2 0.7 multiply_reduce_fusion
  31.9 5.6 %fusion.34 = f32[16,2,1,1024]{3,2,1,0:T(1,128)S(1)} fusion(bf16[16,2,1024,128]{3,2,1,0:T(8,128)(2,1)} %param.24, bf16[16,2,128,1]{2,1,0,3:T(2,128)(2,1)S(1)} %get-tuple-element.12), kind=kOutput, calls=%fused_computation.48 | convolution fusion | flops 8388608 | bytes 8527872 | tf_op jit(solution)/shard_map/shd,shld->shl/dot_general | solution.py:26
  37.6 0.0 copy-start.14
  37.6 0.0 copy-start.10
  37.6 0.0 copy-start.8
  37.6 0.0 copy-start.6
  37.6 0.3 fusion.72
  37.9 0.3 fusion.32
  38.2 0.3 fusion.26
  38.5 0.3 convolution_convert_fusion.1
  38.8 0.0 copy-start.7
  38.8 0.0 copy-start.1
  38.8 0.0 copy-start.2
  38.9 0.0 copy-start.13
  38.9 4.7 %fusion.24 = f32[16,2,1,128]{3,2,1,0:T(1,128)S(1)} fusion(bf16[16,2,1024,128]{3,2,1,0:T(8,128)(2,1)} %param.25, bf16[16,2,1024,1]{2,1,0,3:T(2,128)(2,1)S(1)} %fusion.26), kind=kOutput, calls=%fused_computation.33 | convolution fusion | flops 8388608 | bytes 8470528 | tf_op jit(solution)/shard_map/shl,shld->shd/dot_general | solution.py:42
  43.6 0.1 add_convert_fusion.1
  43.7 2.1 %fusion.46 = f32[16,2048]{1,0:T(8,128)} fusion(bf16[256,2048]{1,0:T(8,128)(2,1)} %param.34, bf16[2,8,2,128]{3,2,1,0:T(2,128)(2,1)S(1)} %bitcast.56), kind=kOutput, calls=%fused_computation.66 | convolution fusion | flops 16777216 | bytes 1187840 | tf_op jit(solution)/shard_map/dot_general | solution.py:100
  45.8 0.0 reduce-scatter.4.cloned.1.call-update
  45.8 0.1 fusion.53
  45.9 0.2 select_reduce_fusion.2
  46.2 0.1 convolution_convert_fusion.2
  46.3 0.1 all_to_all.25
  46.4 0.6 copy.49
  47.0 3.7 %all-to-all-start.1 = ((bf16[4,8,4]{1,2,0:T(4,128)(2,1)}), bf16[4,8,4]{1,2,0:T(4,128)(2,1)S(1)}, u32[]{:S(2)}, u32[]{:S(2)}) async-start(bf16[4,8,4]{1,2,0:T(4,128)(2,1)} %copy.49), calls=%async_computation.2 | async-start | bytes 8192 | tf_op jit(solution)/shard_map/all_to_all | solution.py:128
  50.8 26.8 %reduce-scatter.4.cloned.1.call-done = f32[16,256]{1,0:T(8,128)} async-done(((f32[16,2048]{1,0:T(8,128)}), f32[16,256]{1,0:T(8,128)}) %reduce-scatter.4.cloned.1.call-update) | async-done | bytes 16400 | tf_op jit(solution)/shard_map/reduce_scatter | solution.py:105
  77.6 0.7 add_convert_fusion
  78.3 13.9 %all_gather.7 = bf16[16,2048]{1,0:T(8,128)(2,1)S(1)} all-gather(bf16[16,256]{1,0:T(8,128)(2,1)S(1)} %add_convert_fusion), channel_id=1, replica_groups=mesh['ep'=4,'tp'=8] {'tp'}, dimensions={1}, use_global_device_ids=true | all-gather | bytes 73728 | tf_op jit(solution)/shard_map/all_gather | solution.py:107
  92.2 0.1 fusion.15
  92.4 0.9 fusion
  93.2 3.6 %all-to-all-start = ((bf16[4,8,2048]{2,1,0:T(8,128)(2,1)}), bf16[4,8,2048]{2,1,0:T(8,128)(2,1)S(1)}, u32[]{:S(2)}, u32[]{:S(2)}) async-start(bf16[4,8,2048]{2,1,0:T(8,128)(2,1)} %fusion), calls=%async_computation.1 | async-start | bytes 262144 | tf_op jit(solution)/shard_map/all_to_all | solution.py:127
  96.9 0.1 select_reduce_fusion.1
  97.0 0.1 mul.181
  97.1 4.8 %all-to-all-done = bf16[4,8,2048]{2,1,0:T(8,128)(2,1)S(1)} async-done(((bf16[4,8,2048]{2,1,0:T(8,128)(2,1)}), bf16[4,8,2048]{2,1,0:T(8,128)(2,1)S(1)}, u32[]{:S(2)}, u32[]{:S(2)}) %all-to-all-start) | async-done | bytes 131104 | tf_op jit(solution)/shard_map/all_to_all | solution.py:127
  101.9 1.5 fusion.10
  103.4 0.0 copy-done
  103.4 2.7 %fusion.4 = f32[32,2048]{1,0:T(8,128)} fusion(bf16[1,256,2048]{2,1,0:T(8,128)(2,1)S(1)} %copy-done, bf16[1,2048,256]{2,1,0:T(8,128)(2,1)} %param.41, bf16[4,8,2048]{2,1,0:T(8,128)(2,1)S(1)} %all-to-all-done, f32[32,256]{1,0:T(8,128)S(1)} %fusion.10, f32[32]{0:T(128)S(1)} %mul.181), kind=kOutput, calls=%fused_computation.7 | convolution fusion | flops 67166208 | bytes 2523264 | tf_op jit(solution)/shard_map/dot_general | solution.py:143
  106.1 0.0 reduce-scatter.6.cloned.1.call-update
  106.1 0.0 reduce-scatter.8.cloned.1.call-start
  106.2 1.5 fusion.44
  107.6 0.0 reduce-scatter.8.cloned.1.call-update
  107.7 26.1 %reduce-scatter.6.cloned.1.call-done = f32[32,256]{1,0:T(8,128)} async-done(((f32[32,2048]{1,0:T(8,128)}), f32[32,256]{1,0:T(8,128)}) %reduce-scatter.6.cloned.1.call-update) | async-done | bytes 32784 | tf_op jit(solution)/shard_map/reduce_scatter | solution.py:145
  133.7 1.4 convert_bitcast_fusion
  135.1 3.6 %all-to-all-start.2 = ((bf16[4,8,256]{2,1,0:T(8,128)(2,1)}), bf16[4,8,256]{2,1,0:T(8,128)(2,1)S(1)}, u32[]{:S(2)}, u32[]{:S(2)}) async-start(bf16[4,8,256]{2,1,0:T(8,128)(2,1)} %convert_bitcast_fusion), calls=%async_computation.4 | async-start | bytes 32768 | tf_op jit(solution)/shard_map/all_to_all | solution.py:148
  138.7 26.0 %reduce-scatter.8.cloned.1.call-done = f32[16,256]{1,0:T(8,128)} async-done(((f32[16,2048]{1,0:T(8,128)}), f32[16,256]{1,0:T(8,128)}) %reduce-scatter.8.cloned.1.call-update) | async-done | bytes 16400 | tf_op jit(solution)/shard_map/reduce_scatter | solution.py:146
  164.7 1.5 fusion.5
  (35 shorter events, 0.2 us)
Async XLA Ops:
  7.2 96.2 %copy-start = (bf16[1,256,2048]{2,1,0:T(8,128)(2,1)S(1)}, bf16[1,256,2048]{2,1,0:T(8,128)(2,1)}, u32[]{:S(2)}) copy-start(bf16[1,256,2048]{2,1,0:T(8,128)(2,1)} %param.42) | copy-start | bytes 3145732
  7.2 31.3 %copy-start.5 = (f32[2048]{0:T(1024)S(1)}, f32[2048]{0:T(1024)}, u32[]{:S(2)}) copy-start(f32[2048]{0:T(1024)} %param.28) | copy-start | bytes 24580
  7.2 30.3 %copy-start.4 = (f32[16,2,1024]{2,1,0:T(2,128)S(1)}, f32[16,2,1024]{2,1,0:T(2,128)}, u32[]{:S(2)}) copy-start(f32[16,2,1024]{2,1,0:T(2,128)} %param.26) | copy-start | bytes 393220
  7.2 31.3 %copy-start.3 = (bf16[2048,256]{1,0:T(8,128)(2,1)S(1)}, bf16[2048,256]{1,0:T(8,128)(2,1)}, u32[]{:S(2)}) copy-start(bf16[2048,256]{1,0:T(8,128)(2,1)} %param.31) | copy-start | bytes 3145732
  7.2 70.3 %reduce-scatter.4.cloned.1.call-start = ((), (), s32[]{:S(2)}) async-start(), calls=%async_computation.6 | async-start | bytes 147456 | tf_op jit(solution)/shard_map/reduce_scatter | solution.py:105
  31.1 12.5 %copy-start.11 = (f32[16,2]{0,1:T(2,128)}, f32[16,2]{0,1:T(2,128)S(1)}, u32[]{:S(2)}) copy-start(f32[16,2]{0,1:T(2,128)S(1)} %fusion.58) | copy-start | bytes 388
  37.5 8.3 %copy-start.9 = (s32[16,1]{0,1:T(1,128)S(1)}, s32[16,1]{0,1:T(1,128)}, u32[]{:S(2)}) copy-start(s32[16,1]{0,1:T(1,128)} %param.36) | copy-start | bytes 196
  37.5 8.6 %copy-start.12 = (f32[16,2]{0,1:T(2,128)S(1)}, f32[16,2]{0,1:T(2,128)}, u32[]{:S(2)}) copy-start(f32[16,2]{0,1:T(2,128)} %param.39) | copy-start | bytes 388
  37.6 8.6 %copy-start.14 = (f32[16]{0:T(128)S(1)}, f32[16]{0:T(128)}, u32[]{:S(2)}) copy-start(f32[16]{0:T(128)} %param.38) | copy-start | bytes 196
  37.6 8.6 %copy-start.10 = (s32[16,2]{0,1:T(2,128)S(1)}, s32[16,2]{0,1:T(2,128)}, u32[]{:S(2)}) copy-start(s32[16,2]{0,1:T(2,128)} %param.37) | copy-start | bytes 388
  37.6 40.0 %copy-start.8 = (bf16[16,256]{1,0:T(8,128)(2,1)S(1)}, bf16[16,256]{1,0:T(8,128)(2,1)}, u32[]{:S(2)}) copy-start(bf16[16,256]{1,0:T(8,128)(2,1)} %param.23) | copy-start | bytes 24580
  37.6 54.8 %copy-start.6 = (f32[2048]{0:T(1024)S(1)}, f32[2048]{0:T(1024)}, u32[]{:S(2)}) copy-start(f32[2048]{0:T(1024)} %param.35) | copy-start | bytes 24580
  38.8 67.3 %copy-start.7 = (bf16[16,2,128]{2,1,0:T(2,128)(2,1)}, bf16[16,2,128]{2,1,0:T(2,128)(2,1)S(1)}, u32[]{:S(2)}) copy-start(bf16[16,2,128]{2,1,0:T(2,128)(2,1)S(1)} %convert_element_type.102) | copy-start | bytes 24580
  38.8 67.3 %copy-start.1 = (bf16[256,2048]{1,0:T(8,128)(2,1)S(1)}, bf16[256,2048]{1,0:T(8,128)(2,1)}, u32[]{:S(2)}) copy-start(bf16[256,2048]{1,0:T(8,128)(2,1)} %param.44) | copy-start | bytes 3145732
  38.8 67.3 %copy-start.2 = (bf16[2048,256]{1,0:T(8,128)(2,1)S(1)}, bf16[2048,256]{1,0:T(8,128)(2,1)}, u32[]{:S(2)}) copy-start(bf16[2048,256]{1,0:T(8,128)(2,1)} %param.43) | copy-start | bytes 3145732
  38.9 99.9 %copy-start.13 = (f32[256]{0:T(256)S(1)}, f32[256]{0:T(256)}, u32[]{:S(2)}) copy-start(f32[256]{0:T(256)} %param.45) | copy-start | bytes 3076
  47.0 46.2 %all-to-all-start.1 = ((bf16[4,8,4]{1,2,0:T(4,128)(2,1)}), bf16[4,8,4]{1,2,0:T(4,128)(2,1)S(1)}, u32[]{:S(2)}, u32[]{:S(2)}) async-start(bf16[4,8,4]{1,2,0:T(4,128)(2,1)} %copy.49), calls=%async_computation.2 | async-start | bytes 8192 | tf_op jit(solution)/shard_map/all_to_all | solution.py:128
  93.2 8.7 %all-to-all-start = ((bf16[4,8,2048]{2,1,0:T(8,128)(2,1)}), bf16[4,8,2048]{2,1,0:T(8,128)(2,1)S(1)}, u32[]{:S(2)}, u32[]{:S(2)}) async-start(bf16[4,8,2048]{2,1,0:T(8,128)(2,1)} %fusion), calls=%async_computation.1 | async-start | bytes 262144 | tf_op jit(solution)/shard_map/all_to_all | solution.py:127
  96.9 36.9 %reduce-scatter.6.cloned.1.call-start = ((), (), s32[]{:S(2)}) async-start(), calls=%async_computation.7 | async-start | bytes 294912 | tf_op jit(solution)/shard_map/reduce_scatter | solution.py:145
  106.1 58.6 %reduce-scatter.8.cloned.1.call-start = ((), (), s32[]{:S(2)}) async-start(), calls=%async_computation.8 | async-start | bytes 147456 | tf_op jit(solution)/shard_map/reduce_scatter | solution.py:146
  135.1 29.6 %all-to-all-start.2 = ((bf16[4,8,256]{2,1,0:T(8,128)(2,1)}), bf16[4,8,256]{2,1,0:T(8,128)(2,1)S(1)}, u32[]{:S(2)}, u32[]{:S(2)}) async-start(bf16[4,8,256]{2,1,0:T(8,128)(2,1)} %convert_bitcast_fusion), calls=%async_computation.4 | async-start | bytes 32768 | tf_op jit(solution)/shard_map/all_to_all | solution.py:148
Sparse Core Ops, SparseCore 0:
  45.9 31.5 reduce-scatter.3
  106.2 27.4 reduce-scatter.5
  136.0 28.7 reduce-scatter.7
where the time goes:
time: 174 us; the launch traced here: 173 us
  waiting for transfers between devices  83.8 us (48%)
  blocking collectives  29.8 us (17%)
  matrix products  24.9 us (14%)
  between operations  14 us (8%)
  starting transfers between devices  11 us (6%)
  other arithmetic  7.35 us (4%)
  local copies, waits for them, and re-layouts  1.82 us (1%)
    reduce_scatter x1, waiting for transfers between devices, body(): lax.psum_scatter(partial_value, 'tp', scatter_dimension=1, tiled=True)  26.8 us
    reduce_scatter x1, waiting for transfers between devices, body(): lax.psum_scatter(expert_part, 'tp', scatter_dimension=1, tiled=True)  26.1 us
    reduce_scatter x1, waiting for transfers between devices, body(): lax.psum_scatter(dense_part, 'tp', scatter_dimension=1, tiled=True)  26 us
    all_gather x1, blocking collectives, body(): gathered = lax.all_gather(tokens, 'tp', axis=1, tiled=True)  15.9 us
    all_gather x1, blocking collectives, body(): lax.all_gather(own_residual, 'tp', axis=1, tiled=True)  13.9 us
    dot_general x1, matrix products, attend(): jnp.einsum('shd,shld->shl', queries, key_cache, preferred_element_type=jn...  5.63 us
    all_to_all x1, waiting for transfers between devices, body(): lax.all_to_all(send_rows, 'ep', split_axis=0, concat_axis=0, tiled=True)  4.85 us
    dot_general x1, matrix products, attend(): jnp.einsum('shl,shld->shd', weights, value_cache, preferred_element_type=...  4.72 us
  transfers between devices with their start and end apart: 6, of which 4 were waited for; matrix products, arithmetic and copies ran while one was open for 3% of the time, Pallas kernels for 0%

commit v1 on v0

--- a/solution.py
+++ b/solution.py
@@ -7,6 +7,23 @@
 EPG = 4
 EPS = 1e-06
 FLOOR = -1e30
+
+
+def in_order(blocks, dim):
+    blocks = jnp.moveaxis(blocks, 0, dim)
+    lengths = blocks.shape
+    return blocks.reshape(*lengths[:dim], lengths[dim] * lengths[dim + 1], *lengths[dim + 2 :])
+
+
+def collect(value, axis, dim):
+    size = lax.axis_size(axis)
+    forward = [(i, (i + 1) % size) for i in range(size)]
+    pieces = [value]
+    while len(pieces) < size:
+        pieces.append(lax.ppermute(pieces[-1], axis, forward))
+    index = lax.axis_index(axis)
+    pieces = jnp.stack(pieces)[(index - jnp.arange(size)) % size]
+    return in_order(pieces, dim)
 
 
 def norm_rows(row_data, gain_vec):
@@ -104,7 +121,7 @@
     )
     piece_sum = lax.psum_scatter(partial_value, "tp", scatter_dimension=1, tiled=True)
     own_residual = (tokens.astype(jnp.float32) + piece_sum).astype(jnp.bfloat16)
-    moe_in = norm_rows(lax.all_gather(own_residual, "tp", axis=1, tiled=True), moe_gain)
+    moe_in = norm_rows(collect(own_residual, "tp", 1), moe_gain)
     groups = lax.axis_size("ep")
     capacity = max(2, 2 * seq_count // groups)
     first_share = jax.nn.sigmoid(pair_logits[:, 0] - pair_logits[:, 1])

time: 174 us -> 192 us (1.10)
  waiting for transfers between devices: 83.8 us -> 116 us
  blocking collectives: 29.8 us -> 15.9 us
    ppermute x0 -> x7, waiting for transfers between devices: none -> 34.1 us  [collect(): pieces.append(lax.ppermute(pieces[-1], axis, forward))]
    all_gather x1 -> x0, blocking collectives: 13.9 us -> none  [body(): lax.all_gather(own_residual, 'tp', axis=1, tiled=True)]
  transfers between devices with their start and end apart: 6 -> 13, of which waited for: 4 -> 11; matrix products, arithmetic and copies ran while one was open for 3% -> 4% of each run, Pallas kernels for 0% -> 0%
where the time goes in v1:
time: 192 us; the launch traced here: 191 us
  waiting for transfers between devices  116 us (60%)
  matrix products  23.9 us (12%)
  blocking collectives  15.9 us (8%)
  between operations  14.1 us (7%)
  starting transfers between devices  11 us (6%)
  other arithmetic  7.33 us (4%)
  local copies, waits for them, and re-layouts  2.38 us (1%)
    ppermute x7, waiting for transfers between devices, collect(): pieces.append(lax.ppermute(pieces[-1], axis, forward))  34.1 us
    reduce_scatter x1, waiting for transfers between devices, body(): lax.psum_scatter(partial_value, 'tp', scatter_dimension=1, tiled=True)  26.8 us
    reduce_scatter x1, waiting for transfers between devices, body(): lax.psum_scatter(dense_part, 'tp', scatter_dimension=1, tiled=True)  25.9 us
    reduce_scatter x1, waiting for transfers between devices, body(): lax.psum_scatter(expert_part, 'tp', scatter_dimension=1, tiled=True)  24.6 us
    all_gather x1, blocking collectives, body(): gathered = lax.all_gather(tokens, 'tp', axis=1, tiled=True)  15.9 us
    dot_general x1, matrix products, attend(): jnp.einsum('shd,shld->shl', queries, key_cache, preferred_element_type=jn...  5.63 us
    all_to_all x1, waiting for transfers between devices, body(): lax.all_to_all(send_rows, 'ep', split_axis=0, concat_axis=0, tiled=True)  4.85 us
    dot_general x1, matrix products, attend(): jnp.einsum('shl,shld->shd', weights, value_cache, preferred_element_type=...  4.58 us
  transfers between devices with their start and end apart: 13, of which 11 were waited for; matrix products, arithmetic and copies ran while one was open for 4% of the time, Pallas kernels for 0%

profile of v1, /device:TPU:0, one launch (start us, length us, event | category | flops | bytes accessed | tf_op | source)
XLA Modules:
  0.0 190.8 jit_solution(7869532155157101747)
XLA Ops:
  7.2 0.0 copy-start
  7.2 0.0 copy-start.4
  7.2 0.0 reduce-scatter.4.cloned.1.call-start
  7.3 0.8 broadcast_add_fusion
  8.0 0.7 iota_compare_fusion.1
  8.7 15.9 %all_gather.3 = bf16[16,2048]{1,0:T(8,128)(2,1)S(1)} all-gather(bf16[16,256]{1,0:T(8,128)(2,1)} %param.23), channel_id=1, replica_groups=mesh['ep'=4,'tp'=8] {'tp'}, dimensions={1}, use_global_device_ids=true | all-gather | bytes 73728 | tf_op jit(solution)/shard_map/all_gather | solution.py:91
  24.6 0.1 fusion.12
  24.8 1.5 fusion.61
  26.3 0.1 multiply_reduce_fusion.1
  26.4 1.5 fusion.64
  28.0 0.1 multiply_reduce_fusion.2
  28.1 0.1 iota_compare_fusion
  28.1 1.1 select_reduce_fusion
  29.2 0.1 copy.52
  29.3 0.7 dynamic_slice.7
  30.0 1.0 fusion.49
  31.0 0.0 copy-start.11
  31.0 0.1 copy.53
  31.1 0.7 multiply_reduce_fusion
  31.8 5.6 %fusion.32 = f32[16,2,1,1024]{3,2,1,0:T(1,128)S(1)} fusion(bf16[16,2,1024,128]{3,2,1,0:T(8,128)(2,1)} %param.24, bf16[16,2,128,1]{2,1,0,3:T(2,128)(2,1)S(1)} %get-tuple-element.14), kind=kOutput, calls=%fused_computation.56 | convolution fusion | flops 8388608 | bytes 8527872 | tf_op jit(solution)/shard_map/shd,shld->shl/dot_general | solution.py:43
  37.5 0.0 copy-start.12
  37.5 0.3 fusion.66
  37.9 0.3 fusion.30
  38.2 0.3 fusion.24
  38.5 0.3 convolution_convert_fusion.1
  38.8 0.0 copy-start.7
  38.8 4.6 %fusion.22 = f32[16,2,1,128]{3,2,1,0:T(1,128)S(1)} fusion(bf16[16,2,1024,128]{3,2,1,0:T(8,128)(2,1)} %param.25, bf16[16,2,1024,1]{2,1,0,3:T(2,128)(2,1)S(1)} %fusion.24), kind=kOutput, calls=%fused_computation.32 | convolution fusion | flops 8388608 | bytes 8470528 | tf_op jit(solution)/shard_map/shl,shld->shd/dot_general | solution.py:59
  43.4 0.1 add_convert_fusion.1
  43.5 0.9 fusion.37
  44.4 0.0 reduce-scatter.4.cloned.1.call-update
  44.4 0.1 fusion.44
  44.5 0.2 select_reduce_fusion.2
  44.8 0.1 convolution_convert_fusion.2
  44.9 0.1 all_to_all.25
  45.0 0.6 copy.57
  45.6 3.7 %all-to-all-start.1 = ((bf16[4,8,4]{1,2,0:T(4,128)(2,1)}), bf16[4,8,4]{1,2,0:T(4,128)(2,1)S(1)}, u32[]{:S(2)}, u32[]{:S(2)}) async-start(bf16[4,8,4]{1,2,0:T(4,128)(2,1)} %copy.57), calls=%async_computation.2 | async-start | bytes 8192 | tf_op jit(solution)/shard_map/all_to_all | solution.py:145
  49.4 26.8 %reduce-scatter.4.cloned.1.call-done = f32[16,256]{1,0:T(8,128)} async-done(((f32[16,2048]{1,0:T(8,128)}), f32[16,256]{1,0:T(8,128)}) %reduce-scatter.4.cloned.1.call-update) | async-done | bytes 16400 | tf_op jit(solution)/shard_map/reduce_scatter | solution.py:122
  76.1 0.7 constant_dynamic-update-slice_fusion.7
  76.9 4.9 %collective-permute-done = bf16[16,256]{1,0:T(8,128)(2,1)S(1)} collective-permute-done((bf16[16,256]{1,0:T(8,128)(2,1)S(1)}, bf16[16,256]{1,0:T(8,128)(2,1)S(1)}, u32[]{:S(2)}, u32[]{:S(2)}) %collective-permute-start) | collective-permute-done | bytes 8224 | tf_op jit(solution)/shard_map/ppermute | solution.py:23
  81.7 4.9 %collective-permute-done.1 = bf16[16,256]{1,0:T(8,128)(2,1)S(1)} collective-permute-done((bf16[16,256]{1,0:T(8,128)(2,1)S(1)}, bf16[16,256]{1,0:T(8,128)(2,1)S(1)}, u32[]{:S(2)}, u32[]{:S(2)}) %collective-permute-start.1) | collective-permute-done | bytes 8224 | tf_op jit(solution)/shard_map/ppermute | solution.py:23
  86.6 4.9 %collective-permute-done.2 = bf16[16,256]{1,0:T(8,128)(2,1)S(1)} collective-permute-done((bf16[16,256]{1,0:T(8,128)(2,1)S(1)}, bf16[16,256]{1,0:T(8,128)(2,1)S(1)}, u32[]{:S(2)}, u32[]{:S(2)}) %collective-permute-start.2) | collective-permute-done | bytes 8224 | tf_op jit(solution)/shard_map/ppermute | solution.py:23
  91.5 4.9 %collective-permute-done.3 = bf16[16,256]{1,0:T(8,128)(2,1)S(1)} collective-permute-done((bf16[16,256]{1,0:T(8,128)(2,1)S(1)}, bf16[16,256]{1,0:T(8,128)(2,1)S(1)}, u32[]{:S(2)}, u32[]{:S(2)}) %collective-permute-start.3) | collective-permute-done | bytes 8224 | tf_op jit(solution)/shard_map/ppermute | solution.py:23
  96.4 4.9 %collective-permute-done.4 = bf16[16,256]{1,0:T(8,128)(2,1)S(1)} collective-permute-done((bf16[16,256]{1,0:T(8,128)(2,1)S(1)}, bf16[16,256]{1,0:T(8,128)(2,1)S(1)}, u32[]{:S(2)}, u32[]{:S(2)}) %collective-permute-start.4) | collective-permute-done | bytes 8224 | tf_op jit(solution)/shard_map/ppermute | solution.py:23
  101.2 4.9 %collective-permute-done.5 = bf16[16,256]{1,0:T(8,128)(2,1)S(1)} collective-permute-done((bf16[16,256]{1,0:T(8,128)(2,1)S(1)}, bf16[16,256]{1,0:T(8,128)(2,1)S(1)}, u32[]{:S(2)}, u32[]{:S(2)}) %collective-permute-start.5) | collective-permute-done | bytes 8224 | tf_op jit(solution)/shard_map/ppermute | solution.py:23
  106.1 4.9 %collective-permute-done.6 = bf16[16,256]{1,0:T(8,128)(2,1)S(1)} collective-permute-done((bf16[16,256]{1,0:T(8,128)(2,1)S(1)}, bf16[16,256]{1,0:T(8,128)(2,1)S(1)}, u32[]{:S(2)}, u32[]{:S(2)}) %collective-permute-start.6) | collective-permute-done | bytes 8224 | tf_op jit(solution)/shard_map/ppermute | solution.py:23
  111.0 0.5 gather_fusion
  111.6 0.1 fusion.15
  111.7 0.9 fusion
  112.6 3.6 %all-to-all-start = ((bf16[4,8,2048]{2,1,0:T(8,128)(2,1)}), bf16[4,8,2048]{2,1,0:T(8,128)(2,1)S(1)}, u32[]{:S(2)}, u32[]{:S(2)}) async-start(bf16[4,8,2048]{2,1,0:T(8,128)(2,1)} %fusion), calls=%async_computation.1 | async-start | bytes 262144 | tf_op jit(solution)/shard_map/all_to_all | solution.py:144
  116.2 0.1 select_reduce_fusion.1
  116.3 0.1 mul.183
  116.4 4.8 %all-to-all-done = bf16[4,8,2048]{2,1,0:T(8,128)(2,1)S(1)} async-done(((bf16[4,8,2048]{2,1,0:T(8,128)(2,1)}), bf16[4,8,2048]{2,1,0:T(8,128)(2,1)S(1)}, u32[]{:S(2)}, u32[]{:S(2)}) %all-to-all-start) | async-done | bytes 131104 | tf_op jit(solution)/shard_map/all_to_all | solution.py:144
  121.3 0.3 fusion.10
  121.5 0.0 copy-done.7
  121.6 2.7 %fusion.4 = f32[32,2048]{1,0:T(8,128)} fusion(bf16[1,256,2048]{2,1,0:T(8,128)(2,1)S(1)} %copy-done, bf16[1,2048,256]{2,1,0:T(8,128)(2,1)} %param.41, bf16[4,8,2048]{2,1,0:T(8,128)(2,1)S(1)} %all-to-all-done, f32[32,256]{1,0:T(8,128)S(1)} %fusion.10, f32[32]{0:T(128)S(1)} %mul.183), kind=kOutput, calls=%fused_computation.8 | convolution fusion | flops 67166208 | bytes 2523264 | tf_op jit(solution)/shard_map/dot_general | solution.py:160
  124.2 0.0 reduce-scatter.6.cloned.1.call-update
  124.3 0.0 reduce-scatter.8.cloned.1.call-start
  124.3 3.0 %fusion.36 = f32[16,2048]{1,0:T(8,128)} fusion(bf16[256,2048]{1,0:T(8,128)(2,1)} %param.44, bf16[2048,256]{1,0:T(8,128)(2,1)} %param.43, f32[16,2048]{1,0:T(8,128)S(1)} %bitcast.78, f32[2048]{0:T(1024)S(1)} %copy-done.8, f32[16]{0:T(128)S(1)} %add_rsqrt_fusion.2), kind=kOutput, calls=%fused_computation.70 | convolution fusion | flops 33673216 | bytes 2367552 | tf_op jit(solution)/shard_map/dot_general | solution.py:150
  127.3 0.0 reduce-scatter.8.cloned.1.call-update
  127.3 24.6 %reduce-scatter.6.cloned.1.call-done = f32[32,256]{1,0:T(8,128)} async-done(((f32[32,2048]{1,0:T(8,128)}), f32[32,256]{1,0:T(8,128)}) %reduce-scatter.6.cloned.1.call-update) | async-done | bytes 32784 | tf_op jit(solution)/shard_map/reduce_scatter | solution.py:162
  151.9 1.4 convert_bitcast_fusion.1
  153.3 3.6 %all-to-all-start.2 = ((bf16[4,8,256]{2,1,0:T(8,128)(2,1)}), bf16[4,8,256]{2,1,0:T(8,128)(2,1)S(1)}, u32[]{:S(2)}, u32[]{:S(2)}) async-start(bf16[4,8,256]{2,1,0:T(8,128)(2,1)} %convert_bitcast_fusion.1), calls=%async_computation.4 | async-start | bytes 32768 | tf_op jit(solution)/shard_map/all_to_all | solution.py:165
  156.8 25.9 %reduce-scatter.8.cloned.1.call-done = f32[16,256]{1,0:T(8,128)} async-done(((f32[16,2048]{1,0:T(8,128)}), f32[16,256]{1,0:T(8,128)}) %reduce-scatter.8.cloned.1.call-update) | async-done | bytes 16400 | tf_op jit(solution)/shard_map/reduce_scatter | solution.py:163
  182.8 1.5 fusion.5
  (60 shorter events, 0.3 us)
Async XLA Ops:
  7.2 114.4 %copy-start = (bf16[1,256,2048]{2,1,0:T(8,128)(2,1)S(1)}, bf16[1,256,2048]{2,1,0:T(8,128)(2,1)}, u32[]{:S(2)}) copy-start(bf16[1,256,2048]{2,1,0:T(8,128)(2,1)} %param.42) | copy-start | bytes 3145732
  7.2 31.3 %copy-start.5 = (f32[2048]{0:T(1024)S(1)}, f32[2048]{0:T(1024)}, u32[]{:S(2)}) copy-start(f32[2048]{0:T(1024)} %param.28) | copy-start | bytes 24580
  7.2 30.3 %copy-start.4 = (f32[16,2,1024]{2,1,0:T(2,128)S(1)}, f32[16,2,1024]{2,1,0:T(2,128)}, u32[]{:S(2)}) copy-start(f32[16,2,1024]{2,1,0:T(2,128)} %param.26) | copy-start | bytes 393220
  7.2 68.9 %reduce-scatter.4.cloned.1.call-start = ((), (), s32[]{:S(2)}) async-start(), calls=%async_computation.6 | async-start | bytes 147456 | tf_op jit(solution)/shard_map/reduce_scatter | solution.py:122
  31.0 12.3 %copy-start.11 = (f32[16,2]{0,1:T(2,128)}, f32[16,2]{0,1:T(2,128)S(1)}, u32[]{:S(2)}) copy-start(f32[16,2]{0,1:T(2,128)S(1)} %fusion.49) | copy-start | bytes 388
  31.1 7.3 %copy-start.3 = (bf16[2048,256]{1,0:T(8,128)(2,1)S(1)}, bf16[2048,256]{1,0:T(8,128)(2,1)}, u32[]{:S(2)}) copy-start(bf16[2048,256]{1,0:T(8,128)(2,1)} %param.31) | copy-start | bytes 3145732
  37.5 6.0 %copy-start.1 = (bf16[256,2048]{1,0:T(8,128)(2,1)S(1)}, bf16[256,2048]{1,0:T(8,128)(2,1)}, u32[]{:S(2)}) copy-start(bf16[256,2048]{1,0:T(8,128)(2,1)} %param.34) | copy-start | bytes 3145732
  37.5 6.9 %copy-start.9 = (s32[16,1]{0,1:T(1,128)S(1)}, s32[16,1]{0,1:T(1,128)}, u32[]{:S(2)}) copy-start(s32[16,1]{0,1:T(1,128)} %param.36) | copy-start | bytes 196
  37.5 7.2 %copy-start.12 = (f32[16,2]{0,1:T(2,128)S(1)}, f32[16,2]{0,1:T(2,128)}, u32[]{:S(2)}) copy-start(f32[16,2]{0,1:T(2,128)} %param.39) | copy-start | bytes 388
  37.5 7.2 %copy-start.14 = (f32[16]{0:T(128)S(1)}, f32[16]{0:T(128)}, u32[]{:S(2)}) copy-start(f32[16]{0:T(128)} %param.38) | copy-start | bytes 196
  37.5 7.2 %copy-start.10 = (s32[16,2]{0,1:T(2,128)S(1)}, s32[16,2]{0,1:T(2,128)}, u32[]{:S(2)}) copy-start(s32[16,2]{0,1:T(2,128)} %param.37) | copy-start | bytes 388
  37.5 38.6 %copy-start.6 = (bf16[16,256]{1,0:T(8,128)(2,1)S(1)}, bf16[16,256]{1,0:T(8,128)(2,1)}, u32[]{:S(2)}) copy-start(bf16[16,256]{1,0:T(8,128)(2,1)} %param.23) | copy-start | bytes 24580
  37.9 73.9 %copy-start.8 = (f32[2048]{0:T(1024)S(1)}, f32[2048]{0:T(1024)}, u32[]{:S(2)}) copy-start(f32[2048]{0:T(1024)} %param.35) | copy-start | bytes 24580
  38.5 82.8 %copy-start.2 = (bf16[1,2048,256]{2,1,0:T(8,128)(2,1)S(1)}, bf16[1,2048,256]{2,1,0:T(8,128)(2,1)}, u32[]{:S(2)}) copy-start(bf16[1,2048,256]{2,1,0:T(8,128)(2,1)} %param.40) | copy-start | bytes 3145732
  38.8 82.8 %copy-start.7 = (bf16[16,2,128]{2,1,0:T(2,128)(2,1)}, bf16[16,2,128]{2,1,0:T(2,128)(2,1)S(1)}, u32[]{:S(2)}) copy-start(bf16[16,2,128]{2,1,0:T(2,128)(2,1)S(1)} %convert_element_type.112) | copy-start | bytes 24580
  38.8 118.0 %copy-start.13 = (f32[256]{0:T(256)S(1)}, f32[256]{0:T(256)}, u32[]{:S(2)}) copy-start(f32[256]{0:T(256)} %param.45) | copy-start | bytes 3076
  45.6 67.0 %all-to-all-start.1 = ((bf16[4,8,4]{1,2,0:T(4,128)(2,1)}), bf16[4,8,4]{1,2,0:T(4,128)(2,1)S(1)}, u32[]{:S(2)}, u32[]{:S(2)}) async-start(bf16[4,8,4]{1,2,0:T(4,128)(2,1)} %copy.57), calls=%async_computation.2 | async-start | bytes 8192 | tf_op jit(solution)/shard_map/all_to_all | solution.py:145
  76.9 4.9 %collective-permute-start = (bf16[16,256]{1,0:T(8,128)(2,1)S(1)}, bf16[16,256]{1,0:T(8,128)(2,1)S(1)}, u32[]{:S(2)}, u32[]{:S(2)}) collective-permute-start(bf16[16,256]{1,0:T(8,128)(2,1)S(1)} %get-tuple-element.7), channel_id=1, source_target_pairs={{0,1},{1,2},{2,3},{3,4},{4,5},{5,6},{6,7},{7,0},{8,9},{9,10},{10,1... | collective-permute-start | bytes 24584 | tf_op jit(solution)/shard_map/ppermute | solution.py:23
  81.7 4.9 %collective-permute-start.1 = (bf16[16,256]{1,0:T(8,128)(2,1)S(1)}, bf16[16,256]{1,0:T(8,128)(2,1)S(1)}, u32[]{:S(2)}, u32[]{:S(2)}) collective-permute-start(bf16[16,256]{1,0:T(8,128)(2,1)S(1)} %collective-permute-done), channel_id=1, source_target_pairs={{0,1},{1,2},{2,3},{3,4},{4,5},{5,6},{6,7},{7,0},{8,9},{9,10},{10,1... | collective-permute-start | bytes 24584 | tf_op jit(solution)/shard_map/ppermute | solution.py:23
  86.6 4.9 %collective-permute-start.2 = (bf16[16,256]{1,0:T(8,128)(2,1)S(1)}, bf16[16,256]{1,0:T(8,128)(2,1)S(1)}, u32[]{:S(2)}, u32[]{:S(2)}) collective-permute-start(bf16[16,256]{1,0:T(8,128)(2,1)S(1)} %collective-permute-done.1), channel_id=1, source_target_pairs={{0,1},{1,2},{2,3},{3,4},{4,5},{5,6},{6,7},{7,0},{8,9},{9,10},{10,1... | collective-permute-start | bytes 24584 | tf_op jit(solution)/shard_map/ppermute | solution.py:23
  91.5 4.9 %collective-permute-start.3 = (bf16[16,256]{1,0:T(8,128)(2,1)S(1)}, bf16[16,256]{1,0:T(8,128)(2,1)S(1)}, u32[]{:S(2)}, u32[]{:S(2)}) collective-permute-start(bf16[16,256]{1,0:T(8,128)(2,1)S(1)} %collective-permute-done.2), channel_id=1, source_target_pairs={{0,1},{1,2},{2,3},{3,4},{4,5},{5,6},{6,7},{7,0},{8,9},{9,10},{10,1... | collective-permute-start | bytes 24584 | tf_op jit(solution)/shard_map/ppermute | solution.py:23
  96.4 4.9 %collective-permute-start.4 = (bf16[16,256]{1,0:T(8,128)(2,1)S(1)}, bf16[16,256]{1,0:T(8,128)(2,1)S(1)}, u32[]{:S(2)}, u32[]{:S(2)}) collective-permute-start(bf16[16,256]{1,0:T(8,128)(2,1)S(1)} %collective-permute-done.3), channel_id=1, source_target_pairs={{0,1},{1,2},{2,3},{3,4},{4,5},{5,6},{6,7},{7,0},{8,9},{9,10},{10,1... | collective-permute-start | bytes 24584 | tf_op jit(solution)/shard_map/ppermute | solution.py:23
  101.2 4.9 %collective-permute-start.5 = (bf16[16,256]{1,0:T(8,128)(2,1)S(1)}, bf16[16,256]{1,0:T(8,128)(2,1)S(1)}, u32[]{:S(2)}, u32[]{:S(2)}) collective-permute-start(bf16[16,256]{1,0:T(8,128)(2,1)S(1)} %collective-permute-done.4), channel_id=1, source_target_pairs={{0,1},{1,2},{2,3},{3,4},{4,5},{5,6},{6,7},{7,0},{8,9},{9,10},{10,1... | collective-permute-start | bytes 24584 | tf_op jit(solution)/shard_map/ppermute | solution.py:23
  106.1 4.9 %collective-permute-start.6 = (bf16[16,256]{1,0:T(8,128)(2,1)S(1)}, bf16[16,256]{1,0:T(8,128)(2,1)S(1)}, u32[]{:S(2)}, u32[]{:S(2)}) collective-permute-start(bf16[16,256]{1,0:T(8,128)(2,1)S(1)} %collective-permute-done.5), channel_id=1, source_target_pairs={{0,1},{1,2},{2,3},{3,4},{4,5},{5,6},{6,7},{7,0},{8,9},{9,10},{10,1... | collective-permute-start | bytes 24584 | tf_op jit(solution)/shard_map/ppermute | solution.py:23
  112.6 8.7 %all-to-all-start = ((bf16[4,8,2048]{2,1,0:T(8,128)(2,1)}), bf16[4,8,2048]{2,1,0:T(8,128)(2,1)S(1)}, u32[]{:S(2)}, u32[]{:S(2)}) async-start(bf16[4,8,2048]{2,1,0:T(8,128)(2,1)} %fusion), calls=%async_computation.1 | async-start | bytes 262144 | tf_op jit(solution)/shard_map/all_to_all | solution.py:144
  116.2 35.7 %reduce-scatter.6.cloned.1.call-start = ((), (), s32[]{:S(2)}) async-start(), calls=%async_computation.7 | async-start | bytes 294912 | tf_op jit(solution)/shard_map/reduce_scatter | solution.py:162
  124.3 58.5 %reduce-scatter.8.cloned.1.call-start = ((), (), s32[]{:S(2)}) async-start(), calls=%async_computation.8 | async-start | bytes 147456 | tf_op jit(solution)/shard_map/reduce_scatter | solution.py:163
  153.3 29.5 %all-to-all-start.2 = ((bf16[4,8,256]{2,1,0:T(8,128)(2,1)}), bf16[4,8,256]{2,1,0:T(8,128)(2,1)S(1)}, u32[]{:S(2)}, u32[]{:S(2)}) async-start(bf16[4,8,256]{2,1,0:T(8,128)(2,1)} %convert_bitcast_fusion.1), calls=%async_computation.4 | async-start | bytes 32768 | tf_op jit(solution)/shard_map/all_to_all | solution.py:165
Sparse Core Ops, SparseCore 0:
  44.5 31.5 reduce-scatter.3
  124.4 27.4 reduce-scatter.5
  154.2 28.5 reduce-scatter.7
